TPU v7x, 32 devices: a whole 2x2x4 slice. The times are simulated.
32 devices in a mesh: sp: 4 (over z), dp: 8 (over y, x, core).
Axes of the slice: x: 2, y: 2, z: 4, core: 2. Of those that a mesh axis runs over, the one named last changes fastest.
Arguments:
- tokens: bfloat16 [8, 768, 2048], P('dp', 'sp'), may hold values from -36 to 36
- query_weight: bfloat16 [2048, 2048], P('dp'), may hold values from -0.125 to 0.125
- key_weight: bfloat16 [2048, 512], P('dp'), may hold values from -0.125 to 0.125
- value_weight: bfloat16 [2048, 512], P('dp'), may hold values from -0.125 to 0.125
- forget_weight: bfloat16 [2048, 16], replicated, may hold values from -0.125 to 0.125
- forget_bias: float32 [16], replicated, may hold values from 3.4 to 9
Outputs:
- mixed: bfloat16 [8, 768, 2048], P('dp', 'sp')
All inputs are finite; a program needn't handle non-finite values.
Results may differ from a plain program's by a relative error of at most 0.012.
Values may be sent and summed in bfloat16 or wider, within the bound.
A program may use at most 64 MiB of HBM per device.

v0:
```python
import jax
import jax.numpy as jnp
from jax import lax
from jax.sharding import PartitionSpec as P


def pick_block(length):
    for candidate in (512, 384, 256, 128):
        if length % candidate == 0:
            return candidate
    return length


def on_device(tokens, query_weight, key_weight, value_weight, forget_weight, forget_bias):
    token_rows = tokens[0]
    row_count = token_rows.shape[0]
    sp_count = lax.axis_size("sp")
    head_count = forget_weight.shape[1]
    query_width = query_weight.shape[1]
    key_width = key_weight.shape[1]
    head_dim = query_width // head_count
    key_heads = key_width // head_dim
    pieces = (
        lax.all_gather(query_weight, "dp", axis=0, tiled=True),
        lax.all_gather(key_weight, "dp", axis=0, tiled=True),
        lax.all_gather(value_weight, "dp", axis=0, tiled=True),
    )
    query_rows, key_rows, value_rows = tuple(
        (
            jnp.dot(token_rows, weight_piece, preferred_element_type=jnp.float32)
            for weight_piece in pieces
        )
    )
    query_rows = query_rows.astype(jnp.bfloat16)
    key_rows = key_rows.astype(jnp.bfloat16)
    value_rows = value_rows.astype(jnp.bfloat16)
    gate_input = (
        jnp.dot(token_rows, forget_weight, preferred_element_type=jnp.float32)
        + forget_bias[None, :]
    )
    log_gate = jax.nn.log_sigmoid(gate_input).astype(jnp.bfloat16)
    repeats = max(1, sp_count // key_heads)
    if repeats > 1:
        key_rows = jnp.repeat(key_rows.reshape(row_count, key_heads, head_dim), repeats, axis=1)
        key_rows = key_rows.reshape(row_count, key_heads * repeats * head_dim)
        value_rows = jnp.repeat(value_rows.reshape(row_count, key_heads, head_dim), repeats, axis=1)
        value_rows = value_rows.reshape(row_count, key_heads * repeats * head_dim)
    head_query, head_keys, head_values, head_gates = (
        lax.all_to_all(query_rows, "sp", split_axis=1, concat_axis=0, tiled=True),
        lax.all_to_all(key_rows, "sp", split_axis=1, concat_axis=0, tiled=True),
        lax.all_to_all(value_rows, "sp", split_axis=1, concat_axis=0, tiled=True),
        lax.all_to_all(log_gate, "sp", split_axis=1, concat_axis=0, tiled=True),
    )
    seq_length = head_query.shape[0]
    local_heads = head_count // sp_count
    local_keys = head_keys.shape[1] // head_dim
    group_share = local_heads // local_keys
    decay_sum = jnp.cumsum(head_gates.astype(jnp.float32), axis=0)
    decay_grid = decay_sum.T.reshape(local_keys, group_share, seq_length)
    grouped = head_query.reshape(seq_length, local_keys, group_share, head_dim)
    key_grid = head_keys.reshape(seq_length, local_keys, head_dim)
    value_grid = head_values.reshape(seq_length, local_keys, head_dim)
    block_size = pick_block(seq_length)
    block_count = seq_length // block_size
    score_scale = head_dim ** (-0.5)
    offsets = jnp.arange(block_size, dtype=jnp.int32)

    def query_block(block_index):
        first_row = block_index * block_size
        query_part = lax.dynamic_slice_in_dim(grouped, first_row, block_size, 0)
        query_decay = lax.dynamic_slice_in_dim(decay_grid, first_row, block_size, 2)

        def fill_scores(key_block, buffer):
            key_first = key_block * block_size
            key_part = lax.dynamic_slice_in_dim(key_grid, key_first, block_size, 0)
            key_decay = lax.dynamic_slice_in_dim(decay_grid, key_first, block_size, 2)
            raw_scores = jnp.einsum(
                "qkgd,skd->kgqs", query_part, key_part, preferred_element_type=jnp.float32
            )
            biased = raw_scores * score_scale + query_decay[..., :, None] - key_decay[..., None, :]
            allowed = (key_first + offsets)[None, :] <= (first_row + offsets)[:, None]
            masked = jnp.where(allowed, biased, -jnp.inf)
            return lax.dynamic_update_index_in_dim(buffer, masked, key_block, 0)

        score_buffer = lax.fori_loop(
            0,
            block_index + 1,
            fill_scores,
            jnp.full(
                (block_count, local_keys, group_share, block_size, block_size),
                -jnp.inf,
                jnp.float32,
            ),
        )
        row_max = jnp.max(jnp.max(score_buffer, axis=-1), axis=0)
        row_sum = jnp.sum(
            jnp.sum(jnp.exp(score_buffer - row_max[None, ..., None]), axis=-1), axis=0
        )

        def weighted(key_block, accumulated):
            block_scores = lax.dynamic_index_in_dim(score_buffer, key_block, 0, keepdims=False)
            weights = (jnp.exp(block_scores - row_max[..., None]) / row_sum[..., None]).astype(
                jnp.bfloat16
            )
            value_part = lax.dynamic_slice_in_dim(value_grid, key_block * block_size, block_size, 0)
            return accumulated + jnp.einsum(
                "kgqs,skd->qkgd", weights, value_part, preferred_element_type=jnp.float32
            )

        mixed_block = lax.fori_loop(
            0,
            block_index + 1,
            weighted,
            jnp.zeros((block_size, local_keys, group_share, head_dim), jnp.float32),
        )
        return mixed_block.astype(jnp.bfloat16).reshape(block_size, local_heads * head_dim)

    head_mixed = lax.map(query_block, jnp.arange(block_count, dtype=jnp.int32))
    head_mixed = head_mixed.reshape(seq_length, local_heads * head_dim)
    mixed = lax.all_to_all(head_mixed, "sp", split_axis=0, concat_axis=1, tiled=True)
    return mixed[None]


def solution(mesh):
    placed = (P("dp", "sp", None), P("dp", None), P("dp", None), P("dp", None), P(), P())
    return jax.shard_map(
        on_device, mesh=mesh, in_specs=placed, out_specs=P("dp", "sp", None), check_vma=False
    )
```

profile of v0, /device:TPU:0, one launch (start us, length us, event | category | flops | bytes accessed | tf_op | source)
XLA Modules:
  0.0 229.2 jit_solution(9578474785940461810)
XLA Ops:
  10.5 6.3 %all-to-all-start.1 = ((bf16[192,4,4]{0,2,1:T(4,128)(2,1)}), bf16[192,4,4]{0,2,1:T(4,128)(2,1)S(1)}, u32[]{:S(2)}, u32[]{:S(2)}) async-start(bf16[192,4,4]{0,2,1:T(4,128)(2,1)} %all_to_all.61), calls=%async_computation.1 | async-start | bytes 16384 | tf_op jit(solution)/shard_map/all_to_all | solution.py:52
  16.9 22.9 %all-gather.8.cloned.1.call-done = bf16[2048,512]{1,0:T(8,128)(2,1)} async-done(((bf16[256,512]{1,0:T(8,128)(2,1)}), bf16[2048,512]{1,0:T(8,128)(2,1)}) %all-gather.8.cloned.1.call-update) | async-done | bytes 2097168 | tf_op jit(solution)/shard_map/all_gather | solution.py:26
  42.6 4.6 %all-to-all-start.3 = ((bf16[192,4,128]{2,0,1:T(8,128)(2,1)}), bf16[192,4,128]{2,0,1:T(8,128)(2,1)S(1)}, u32[]{:S(2)}, u32[]{:S(2)}) async-start(bf16[192,4,128]{2,0,1:T(8,128)(2,1)} %bitcast.89), calls=%async_computation.3 | async-start | bytes 393216 | tf_op jit(solution)/shard_map/all_to_all | solution.py:51
  47.2 48.7 %all-gather.4.cloned.1.call-done = bf16[2048,2048]{1,0:T(8,128)(2,1)} async-done(((bf16[256,2048]{1,0:T(8,128)(2,1)}), bf16[2048,2048]{1,0:T(8,128)(2,1)}) %all-gather.4.cloned.1.call-update) | async-done | bytes 8388624 | tf_op jit(solution)/shard_map/all_gather | solution.py:24
  95.9 5.2 %convolution_convert_fusion = bf16[192,2048]{1,0:T(8,128)(2,1)S(1)} fusion(bf16[2048,2048]{1,0:T(8,128)(2,1)} %all-gather.4.cloned.1.call-done, bf16[1,192,2048]{2,1,0:T(8,128)(2,1)S(1)} %copy-done), kind=kOutput, calls=%fused_computation.26 | convolution fusion | flops 1611005952 | bytes 9961472 | tf_op jit(solution)/shard_map/dot_general | solution.py:30
  102.1 4.6 %all-to-all-start = ((bf16[192,4,512]{2,0,1:T(8,128)(2,1)}), bf16[192,4,512]{2,0,1:T(8,128)(2,1)S(1)}, u32[]{:S(2)}, u32[]{:S(2)}) async-start(bf16[192,4,512]{2,0,1:T(8,128)(2,1)} %bitcast.88), calls=%async_computation | async-start | bytes 1572864 | tf_op jit(solution)/shard_map/all_to_all | solution.py:49
  107.9 17.7 %all-gather.6.cloned.1.call-done = bf16[2048,512]{1,0:T(8,128)(2,1)} async-done(((bf16[256,512]{1,0:T(8,128)(2,1)}), bf16[2048,512]{1,0:T(8,128)(2,1)}) %all-gather.6.cloned.1.call-update) | async-done | bytes 2097168 | tf_op jit(solution)/shard_map/all_gather | solution.py:25
  128.5 4.6 %all-to-all-start.2 = ((bf16[192,4,128]{2,0,1:T(8,128)(2,1)}), bf16[192,4,128]{2,0,1:T(8,128)(2,1)S(1)}, u32[]{:S(2)}, u32[]{:S(2)}) async-start(bf16[192,4,128]{2,0,1:T(8,128)(2,1)} %bitcast.90), calls=%async_computation.2 | async-start | bytes 393216 | tf_op jit(solution)/shard_map/all_to_all | solution.py:50
  135.4 5.6 %all-to-all-done.2 = bf16[192,4,128]{2,0,1:T(8,128)(2,1)S(1)} async-done(((bf16[192,4,128]{2,0,1:T(8,128)(2,1)}), bf16[192,4,128]{2,0,1:T(8,128)(2,1)S(1)}, u32[]{:S(2)}, u32[]{:S(2)}) %all-to-all-start.2) | async-done | bytes 196640 | tf_op jit(solution)/shard_map/all_to_all | solution.py:50
  141.0 57.3 %while.39 = (s32[]{:T(128)}, bf16[2,384,512]{2,1,0:T(8,128)(2,1)}, s32[2]{0:T(128)S(1)}, bf16[768,1,4,128]{3,2,0,1:T(4,128)(2,1)}, f32[1,4,768]{2,1,0:T(4,128)S(...) while((s32[]{:T(128)}, bf16[2,384,512]{2,1,0:T(8,128)(2,1)}, ...), condition=%wide.region_9.10_spmd.clone.clone, body=%wide.region_2.0_spmd.clone.clone.sunk | while | flops 310195968 | bytes 35959236 | solution.py:118
  144.0 2.5 %broadcast.53 = f32[2,1,4,384,384]{3,4,2,1,0:T(8,128)} broadcast(f32[]{:T(128)} %constant.52.clone.3..sunk), dimensions={} | broadcast | bytes 4718596 | tf_op jit(solution)/shard_map/broadcast.5
  146.5 2.2 while.40
  148.7 2.6 %reduce_max.20 = f32[4,384]{1,0:T(4,128)S(1)} reduce(f32[2,1,4,384,384]{3,4,2,1,0:T(8,128)} %get-tuple-element.530, f32[]{:T(128)} %constant.52.clone.3..sunk), dimensions={0,1,4}, to_apply=%region_5.5 | reduce | flops 1178112 | bytes 4724740 | tf_op jit(solution)/shard_map/while/body/eval_jaxpr/reduce_max | solution.py:95
  151.3 3.0 %exponential_reduce_fusion.2 = f32[4,384]{1,0:T(4,128)S(1)} fusion(f32[2,1,4,384,384]{3,4,2,1,0:T(8,128)} %get-tuple-element.530, f32[4,384]{1,0:T(4,128)S(1)} %reduce_max.20), kind=kLoop, calls=%fused_computation.22.clone.1 | loop fusion | flops 2357760 | bytes 4730880 | tf_op jit(solution)/shard_map/while/body/eval_jaxpr/reduce_sum | solution.py:96
  155.3 7.4 %while.41 = (s32[]{:T(128)}, f32[384,1,4,128]{0,3,2,1:T(8,128)}, s32[]{:T(128)}, bf16[768,1,128]{0,2,1:T(8,128)(2,1)}, f32[2,1,4,384,384]{3,4,2,1,0:T(8,128)}, /...) while((s32[]{:T(128)}, f32[384,1,4,128]{0,3,2,1:T(8,128)}, ...), condition=%wide.region_8.8_spmd, body=%wide.region_7.7_spmd.sunk | while | flops 152961024 | bytes 13480141 | solution.py:110
  159.1 3.6 %fusion.41 = f32[384,1,4,128]{0,3,2,1:T(8,128)} fusion(f32[384,1,4,128]{0,3,2,1:T(8,128)} %get-tuple-element.539, f32[1,1,4,384,384]{4,3,2,1,0:T(8,128)} %copy.54, f32[4,384]{1,0:T(4,128)S(1)} %bitcast.135, f32[4,384]{1,0:T(4,128)S(1)} %bitcast.131, bf16[768,1,128]{0,2,1:T(8,128)(2,1)} %get-tuple-element.553, s32[]{:T(128)S(6)} %select_n.55), kind=kOutput, calls=%fused_computation.3.clone.1 | convolution fusion | flops 152961024 | bytes 4042756 | tf_op jit(solution)/shard_map/while/body/eval_jaxpr/while/body/kgqs,skd->qkgd/dot_general | solution.py:106
  167.8 2.5 %broadcast.53 = f32[2,1,4,384,384]{3,4,2,1,0:T(8,128)} broadcast(f32[]{:T(128)} %constant.52.clone.3..sunk), dimensions={} | broadcast | bytes 4718596 | tf_op jit(solution)/shard_map/broadcast.5
  170.3 4.4 %while.40 = (s32[]{:T(128)}, f32[2,1,4,384,384]{3,4,2,1,0:T(8,128)}, s32[]{:T(128)}, s32[384]{0:T(512)S(1)}, s32[]{:T(128)}, /*index=5*/bf16[768,1,128]{2,0,1:T(...) while((s32[]{:T(128)}, ...), condition=%wide.region_4.4_spmd.clone, body=%wide.region_3.3_spmd.clone.sunk | while | flops 153502464 | bytes 3178217 | solution.py:85
  174.7 2.6 %reduce_max.20 = f32[4,384]{1,0:T(4,128)S(1)} reduce(f32[2,1,4,384,384]{3,4,2,1,0:T(8,128)} %get-tuple-element.530, f32[]{:T(128)} %constant.52.clone.3..sunk), dimensions={0,1,4}, to_apply=%region_5.5 | reduce | flops 1178112 | bytes 4724740 | tf_op jit(solution)/shard_map/while/body/eval_jaxpr/reduce_max | solution.py:95
  177.3 3.0 %exponential_reduce_fusion.2 = f32[4,384]{1,0:T(4,128)S(1)} fusion(f32[2,1,4,384,384]{3,4,2,1,0:T(8,128)} %get-tuple-element.530, f32[4,384]{1,0:T(4,128)S(1)} %reduce_max.20), kind=kLoop, calls=%fused_computation.22.clone.1 | loop fusion | flops 2357760 | bytes 4730880 | tf_op jit(solution)/shard_map/while/body/eval_jaxpr/reduce_sum | solution.py:96
  181.3 14.9 %while.41 = (s32[]{:T(128)}, f32[384,1,4,128]{0,3,2,1:T(8,128)}, s32[]{:T(128)}, bf16[768,1,128]{0,2,1:T(8,128)(2,1)}, f32[2,1,4,384,384]{3,4,2,1,0:T(8,128)}, /...) while((s32[]{:T(128)}, f32[384,1,4,128]{0,3,2,1:T(8,128)}, ...), condition=%wide.region_8.8_spmd, body=%wide.region_7.7_spmd.sunk | while | flops 152961024 | bytes 13480141 | solution.py:110
  185.1 3.6 %fusion.41 = f32[384,1,4,128]{0,3,2,1:T(8,128)} fusion(f32[384,1,4,128]{0,3,2,1:T(8,128)} %get-tuple-element.539, f32[1,1,4,384,384]{4,3,2,1,0:T(8,128)} %copy.54, f32[4,384]{1,0:T(4,128)S(1)} %bitcast.135, f32[4,384]{1,0:T(4,128)S(1)} %bitcast.131, bf16[768,1,128]{0,2,1:T(8,128)(2,1)} %get-tuple-element.553, s32[]{:T(128)S(6)} %select_n.55), kind=kOutput, calls=%fused_computation.3.clone.1 | convolution fusion | flops 152961024 | bytes 4042756 | tf_op jit(solution)/shard_map/while/body/eval_jaxpr/while/body/kgqs,skd->qkgd/dot_general | solution.py:106
  192.6 3.6 %fusion.41 = f32[384,1,4,128]{0,3,2,1:T(8,128)} fusion(f32[384,1,4,128]{0,3,2,1:T(8,128)} %get-tuple-element.539, f32[1,1,4,384,384]{4,3,2,1,0:T(8,128)} %copy.54, f32[4,384]{1,0:T(4,128)S(1)} %bitcast.135, f32[4,384]{1,0:T(4,128)S(1)} %bitcast.131, bf16[768,1,128]{0,2,1:T(8,128)(2,1)} %get-tuple-element.553, s32[]{:T(128)S(6)} %select_n.55), kind=kOutput, calls=%fused_computation.3.clone.1 | convolution fusion | flops 152961024 | bytes 4042756 | tf_op jit(solution)/shard_map/while/body/eval_jaxpr/while/body/kgqs,skd->qkgd/dot_general | solution.py:106
  198.3 22.2 %all_to_all.77 = bf16[4,192,512]{2,1,0:T(8,128)(2,1)S(1)} all-to-all(bf16[4,192,512]{2,1,0:T(8,128)(2,1)} %bitcast.127), channel_id=1, replica_groups=mesh['sp'=4,'dp'=8] {'sp'}, dimensions={0} | all-to-all | bytes 1572864 | tf_op jit(solution)/shard_map/all_to_all | solution.py:120
  (69 shorter events, 44.2 us)
Async XLA Ops:
  6.5 2.2 copy-start
  6.5 33.2 %all-gather.8.cloned.1.call-start = ((), (), s32[]{:S(2)}) async-start(), calls=%async_computation.7 | async-start | bytes 2359296 | tf_op jit(solution)/shard_map/all_gather | solution.py:26
  7.3 88.7 %all-gather.4.cloned.1.call-start = ((), (), s32[]{:S(2)}) async-start(), calls=%async_computation.5 | async-start | bytes 9437184 | tf_op jit(solution)/shard_map/all_gather | solution.py:24
  8.0 117.6 %all-gather.6.cloned.1.call-start = ((), (), s32[]{:S(2)}) async-start(), calls=%async_computation.6 | async-start | bytes 2359296 | tf_op jit(solution)/shard_map/all_gather | solution.py:25
  10.5 32.1 %all-to-all-start.1 = ((bf16[192,4,4]{0,2,1:T(4,128)(2,1)}), bf16[192,4,4]{0,2,1:T(4,128)(2,1)S(1)}, u32[]{:S(2)}, u32[]{:S(2)}) async-start(bf16[192,4,4]{0,2,1:T(4,128)(2,1)} %all_to_all.61), calls=%async_computation.1 | async-start | bytes 16384 | tf_op jit(solution)/shard_map/all_to_all | solution.py:52
  42.6 59.4 %all-to-all-start.3 = ((bf16[192,4,128]{2,0,1:T(8,128)(2,1)}), bf16[192,4,128]{2,0,1:T(8,128)(2,1)S(1)}, u32[]{:S(2)}, u32[]{:S(2)}) async-start(bf16[192,4,128]{2,0,1:T(8,128)(2,1)} %bitcast.89), calls=%async_computation.3 | async-start | bytes 393216 | tf_op jit(solution)/shard_map/all_to_all | solution.py:51
  102.1 26.5 %all-to-all-start = ((bf16[192,4,512]{2,0,1:T(8,128)(2,1)}), bf16[192,4,512]{2,0,1:T(8,128)(2,1)S(1)}, u32[]{:S(2)}, u32[]{:S(2)}) async-start(bf16[192,4,512]{2,0,1:T(8,128)(2,1)} %bitcast.88), calls=%async_computation | async-start | bytes 1572864 | tf_op jit(solution)/shard_map/all_to_all | solution.py:49
  128.5 12.5 %all-to-all-start.2 = ((bf16[192,4,128]{2,0,1:T(8,128)(2,1)}), bf16[192,4,128]{2,0,1:T(8,128)(2,1)S(1)}, u32[]{:S(2)}, u32[]{:S(2)}) async-start(bf16[192,4,128]{2,0,1:T(8,128)(2,1)} %bitcast.90), calls=%async_computation.2 | async-start | bytes 393216 | tf_op jit(solution)/shard_map/all_to_all | solution.py:50
Sparse Core Ops, SparseCore 0:
  9.2 30.4 all-gather.7
  41.6 54.2 all-gather.3
  97.8 27.7 all-gather.5
where the time goes:
time: 230 us; the launch traced here: 229 us
  waiting for transfers between devices  97 us (42%)
  local copies, waits for them, and re-layouts  31.3 us (14%)
  matrix products  27.6 us (12%)
  blocking collectives  22.2 us (10%)
  starting transfers between devices  20.2 us (9%)
  other arithmetic  15.3 us (7%)
  between operations  13.2 us (6%)
  loops' own time  2.43 us (1%)
    all_gather x1, waiting for transfers between devices, on_device(): lax.all_gather(query_weight, 'dp', axis=0, tiled=True)  48.7 us
    all_gather x1, waiting for transfers between devices, on_device(): lax.all_gather(value_weight, 'dp', axis=0, tiled=True)  22.9 us
    all_to_all x1, blocking collectives, on_device(): lax.all_to_all(head_mixed, 'sp', split_axis=0, concat_axis=1, tiled=True)  22.2 us
    all_gather x1, waiting for transfers between devices, on_device(): lax.all_gather(key_weight, 'dp', axis=0, tiled=True)  17.7 us
    dynamic_slice x6, local copies, waits for them, and re-layouts, weighted(): lax.dynamic_index_in_dim(score_buffer, key_block, 0, keepdims=False)  11.5 us
    dot_general x3, matrix products, weighted(): jnp.einsum('kgqs,skd->qkgd', weights, value_part, preferred_element_type=...  10.8 us
    dot_general x3, matrix products, on_device(): jnp.dot(token_rows, weight_piece, preferred_element_type=jnp.float32)  9.52 us
    another operation x8, local copies, waits for them, and re-layouts  7.22 us
  transfers between devices with their start and end apart: 7, of which 4 were waited for; matrix products, arithmetic and copies ran while one was open for 7% of the time, Pallas kernels for 0%

commit v1 on v0

v1 whole, which is shorter than its diff:
```python
import math

import jax
import jax.numpy as jnp
from jax import lax
from jax.experimental import pallas as pl
from jax.experimental.pallas import tpu as pltpu
from jax.sharding import PartitionSpec as P

MESH = pl.DeviceIdType.MESH
F32 = jnp.float32
BF16 = jnp.bfloat16
NT = (((1,), (1,)), ((), ()))
LOG2E = math.log2(math.e)


def flip(index, mask):
    bit = 1
    while bit <= mask:
        if mask & bit:
            index = index + bit * (1 - 2 * ((index // bit) % 2))
        bit *= 2
    return index


def last_bit(mask, half):
    if mask & 1:
        return 1
    return 1 << (mask.bit_length() - 1) if half == 0 else mask & -mask


def make_kernel(sp_count, dp_count, heads, key_heads, head_dim, rows, shard):
    half_shard = shard // 2
    local_heads = heads // 2
    local_keys = key_heads // 2
    group = heads // key_heads
    kw = local_keys * head_dim
    qw = local_heads * head_dim
    pairs = sp_count // 2
    span = 2 * rows
    bits = [1 << i for i in range(dp_count.bit_length() - 1)]
    masks = sorted(range(1, dp_count), key=lambda m: (bin(m).count("1"), m))
    score_scale = head_dim ** (-0.5) * LOG2E
    tile = 256

    def kernel(x_ref, wq_hbm, wk_hbm, wv_hbm, fw_ref, bias_ref, out_ref,
               xpeer, wkv, wq, qbuf, kvbuf, gbuf, gwide, drow, dcol, osend,
               local_sem, w_send, w_recv, x_sem, g_send, g_recv, kv_send, kv_recv,
               o_send, o_recv):
        s = lax.axis_index("sp")
        d = lax.axis_index("dp")
        parity = s % 2
        pair = s // 2
        peer = s + 1 - 2 * parity

        def own_rows(index):
            return pl.ds(pl.multiple_of(index * shard, shard), shard)

        locals_ = [
            pltpu.make_async_copy(
                wk_hbm.at[:, pl.ds(pl.multiple_of(parity * kw, kw), kw)],
                wkv.at[own_rows(d), pl.ds(0, kw)], local_sem.at[0]),
            pltpu.make_async_copy(
                wv_hbm.at[:, pl.ds(pl.multiple_of(parity * kw, kw), kw)],
                wkv.at[own_rows(d), pl.ds(kw, kw)], local_sem.at[1]),
            pltpu.make_async_copy(
                wq_hbm.at[:, pl.ds(pl.multiple_of(parity * qw, qw), qw)],
                wq.at[own_rows(d), :], local_sem.at[2]),
        ]
        for copy in locals_:
            copy.start()

        barrier = pltpu.get_barrier_semaphore()
        for k in range(1, sp_count):
            pl.semaphore_signal(barrier, inc=1, device_id={"sp": (s + k) % sp_count},
                                device_id_type=MESH)
        for b in bits:
            pl.semaphore_signal(barrier, inc=1, device_id={"dp": flip(d, b)},
                                device_id_type=MESH)
        pl.semaphore_wait(barrier, sp_count - 1 + len(bits))

        x_copy = pltpu.make_async_remote_copy(
            x_ref, xpeer, x_sem.at[0], x_sem.at[1], device_id={"sp": peer}, device_id_type=MESH)
        x_copy.start()

        buffers = (wkv, wq)

        def weight_copy(part, mask, half, bit):
            buffer = buffers[part]
            start = flip(d, mask) * shard + half * half_shard
            where = pl.ds(pl.multiple_of(start, half_shard), half_shard)
            there = mask | bit
            return pltpu.make_async_remote_copy(
                buffer.at[where, :], buffer.at[where, :],
                w_send.at[part, there, half], w_recv.at[part, there, half],
                device_id={"dp": flip(d, bit)}, device_id_type=MESH)

        sent = []

        def send(part, mask, half, bit):
            copy = weight_copy(part, mask, half, bit)
            copy.start()
            sent.append(copy)

        def arrive(part, mask, half):
            bit = last_bit(mask, half)
            start = flip(d, mask) * shard + half * half_shard
            where = pl.ds(pl.multiple_of(start, half_shard), half_shard)
            pltpu.make_async_remote_copy(
                buffers[part].at[where, :], buffers[part].at[where, :],
                w_send.at[part, mask, half], w_recv.at[part, mask, half],
                device_id={"dp": flip(d, bit)}, device_id_type=MESH).wait_recv()
            for b in reversed(bits):
                if not mask & b and last_bit(mask | b, half) == b:
                    send(part, mask, half, b)

        def first_half(bit):
            return 0 if bit == 2 else 1

        def direct(part, turn):
            for b in bits[1:] + bits[:1]:
                send(part, 0, (first_half(b) + turn) % 2, b)

        def order(items):
            return sorted(items, key=lambda mh: bin(mh[0]).count("1"))

        early = [(b, first_half(b)) for b in bits]
        late = [(b, 1 - first_half(b)) for b in bits]
        relayed = [(m, h) for m in masks if bin(m).count("1") > 1 for h in (0, 1)]

        locals_[0].wait()
        locals_[1].wait()
        direct(0, 0)
        direct(0, 1)
        locals_[2].wait()
        direct(1, 0)

        gate = lax.dot_general(fw_ref[...], x_ref[...], NT, preferred_element_type=F32)
        row_id = lax.broadcasted_iota(jnp.int32, (heads, 1), 0)
        bias = jnp.zeros((heads, 1), F32)
        for h in range(heads):
            bias = jnp.where(row_id == h, bias_ref[h], bias)
        gate = gate + bias
        log_gate = jnp.minimum(gate, 0.0) - jnp.log1p(jnp.exp(-jnp.abs(gate)))
        gbuf[s] = log_gate.astype(BF16)
        g_copies = []
        for k in range(1, sp_count):
            copy = pltpu.make_async_remote_copy(
                gbuf.at[s], gbuf.at[s], g_send.at[k], g_recv.at[s],
                device_id={"sp": (s + k) % sp_count}, device_id_type=MESH)
            copy.start()
            g_copies.append(copy)

        for m, h in early + late:
            arrive(0, m, h)
        direct(1, 1)
        for m, h in relayed:
            arrive(0, m, h)

        def project_kv(source, which):
            first = pl.multiple_of(which * rows, rows)

            def one(c, carry):
                cols = pl.ds(pl.multiple_of(c * tile, tile), tile)
                kvbuf[pair, pl.ds(first, rows), cols] = jnp.dot(
                    source[...], wkv[:, cols], preferred_element_type=F32).astype(BF16)
                return carry

            lax.fori_loop(0, 2 * kw // tile, one, 0)

        def kv_copy(source_pair, target_pair, which, part):
            where = pl.ds(pl.multiple_of(which * rows, rows), rows)
            return pltpu.make_async_remote_copy(
                kvbuf.at[source_pair, where], kvbuf.at[source_pair, where],
                kv_send.at[target_pair, part], kv_recv.at[source_pair, part],
                device_id={"sp": target_pair * 2 + parity}, device_id_type=MESH)

        def send_kv(which, part):
            for j in range(1, pairs):
                @pl.when(pair < j)
                def _():
                    kv_copy(pair, j, which, part).start()

        project_kv(x_ref, parity)
        send_kv(parity, 0)
        for m, h in early:
            arrive(1, m, h)

        x_copy.wait_recv()
        project_kv(xpeer, 1 - parity)
        send_kv(1 - parity, 1)

        for k in range(1, sp_count):
            source = (s + k) % sp_count
            pltpu.make_async_remote_copy(
                gbuf.at[source], gbuf.at[source], g_send.at[k], g_recv.at[source],
                device_id={"sp": source}, device_id_type=MESH).wait_recv()
        gwide[...] = gbuf[...].astype(F32)
        mine = pl.ds(pl.multiple_of(parity * local_heads, local_heads), local_heads)
        up_row = lax.broadcasted_iota(jnp.int32, (rows, span), 0)
        up_col = lax.broadcasted_iota(jnp.int32, (rows, span), 1)
        upper_a = jnp.where(up_row <= up_col, 1.0, 0.0).astype(BF16)
        upper_b = jnp.where(up_row + rows <= up_col, 1.0, 0.0).astype(BF16)
        low_row = lax.broadcasted_iota(jnp.int32, (span, rows), 0) + pair * span
        low_col = lax.broadcasted_iota(jnp.int32, (span, rows), 1)
        before = jnp.zeros((local_heads, 1), F32)
        column = jnp.zeros((span, local_heads), F32)
        for j in range(pairs):
            wide_a = gwide[2 * j, mine, :]
            wide_b = gwide[2 * j + 1, mine, :]
            gate_a = wide_a.astype(BF16)
            gate_b = wide_b.astype(BF16)
            inside = (jnp.dot(gate_a, upper_a, preferred_element_type=F32)
                      + jnp.dot(gate_b, upper_b, preferred_element_type=F32))
            drow[j] = (inside + before) * LOG2E
            before = (before + jnp.sum(wide_a, axis=1, keepdims=True)
                      + jnp.sum(wide_b, axis=1, keepdims=True))
            for block, gates in ((2 * j, gate_a), (2 * j + 1, gate_b)):
                lower = jnp.where(low_col + block * rows <= low_row, 1.0, 0.0).astype(BF16)
                column = column + lax.dot_general(lower, gates, NT, preferred_element_type=F32)
        dcol[...] = column * LOG2E

        for m, h in late + relayed:
            arrive(1, m, h)

        def project_q(c, carry):
            cols = pl.ds(pl.multiple_of(c * tile, tile), tile)
            own = pl.ds(pl.multiple_of(parity * rows, rows), rows)
            other = pl.ds(pl.multiple_of((1 - parity) * rows, rows), rows)
            qbuf[own, cols] = jnp.dot(
                x_ref[...], wq[:, cols], preferred_element_type=F32).astype(BF16)
            qbuf[other, cols] = jnp.dot(
                xpeer[...], wq[:, cols], preferred_element_type=F32).astype(BF16)
            return carry

        lax.fori_loop(0, qw // tile, project_q, 0)

        for j in range(pairs - 1):
            @pl.when(j < pair)
            def _():
                kv_copy(j, pair, parity, 0).wait_recv()
                kv_copy(j, pair, 1 - parity, 1).wait_recv()

        def out_copy(head):
            cols = pl.ds(pl.multiple_of(parity * qw + head * head_dim, head_dim), head_dim)
            return pltpu.make_async_remote_copy(
                osend.at[head], out_ref.at[:, cols], o_send.at[head], o_recv.at[head],
                device_id={"sp": peer}, device_id_type=MESH)

        def attend(turn, carry):
            block = (parity + 1 + turn) % 2
            where = pl.ds(pl.multiple_of(block * rows, rows), rows)
            row = lax.broadcasted_iota(jnp.int32, (rows, span), 0) + block * rows
            col = lax.broadcasted_iota(jnp.int32, (rows, span), 1)
            allowed = col <= row
            for head in range(local_heads):
                kh = head // group
                query = qbuf[where, head * head_dim:(head + 1) * head_dim]
                query_decay = dcol[where, head:head + 1]

                def scores(j):
                    key = kvbuf[j, :, kh * head_dim:(kh + 1) * head_dim]
                    raw = lax.dot_general(query, key, NT, preferred_element_type=F32)
                    return raw * score_scale + query_decay - drow[j, head:head + 1, :]

                def values(j):
                    return kvbuf[j, :, kw + kh * head_dim:kw + (kh + 1) * head_dim]

                sc = jnp.where(allowed, scores(pair), -jnp.inf)
                top = jnp.max(sc, axis=1, keepdims=True)
                weight = jnp.exp2(sc - top)
                total = jnp.sum(weight, axis=1, keepdims=True)
                acc = jnp.dot(weight.astype(BF16), values(pair), preferred_element_type=F32)

                def earlier(j, state):
                    top, total, acc = state
                    sc = scores(j)
                    new_top = jnp.maximum(top, jnp.max(sc, axis=1, keepdims=True))
                    keep = jnp.exp2(top - new_top)
                    weight = jnp.exp2(sc - new_top)
                    total = total * keep + jnp.sum(weight, axis=1, keepdims=True)
                    acc = acc * keep + jnp.dot(
                        weight.astype(BF16), values(j), preferred_element_type=F32)
                    return new_top, total, acc

                top, total, acc = lax.fori_loop(0, pair, earlier, (top, total, acc))
                result = (acc / total).astype(BF16)

                @pl.when(turn == 0)
                def _():
                    osend[head] = result
                    out_copy(head).start()

                @pl.when(turn == 1)
                def _():
                    cols = pl.ds(
                        pl.multiple_of(parity * qw + head * head_dim, head_dim), head_dim)
                    out_ref[:, cols] = result
            return carry

        lax.fori_loop(0, 2, attend, 0)

        x_copy.wait_send()
        for copy in sent + g_copies:
            copy.wait_send()
        for j in range(1, pairs):
            @pl.when(pair < j)
            def _():
                kv_copy(pair, j, parity, 0).wait_send()
                kv_copy(pair, j, 1 - parity, 1).wait_send()
        for head in range(local_heads):
            cols = pl.ds(pl.multiple_of((1 - parity) * qw + head * head_dim, head_dim), head_dim)
            out_copy(head).wait_send()
            pltpu.make_async_remote_copy(
                osend.at[head], out_ref.at[:, cols], o_send.at[head], o_recv.at[head],
                device_id={"sp": peer}, device_id_type=MESH).wait_recv()

    model = shard * dp_count
    scratch = [
        pltpu.VMEM((rows, model), BF16),
        pltpu.VMEM((model, 2 * kw), BF16),
        pltpu.VMEM((model, qw), BF16),
        pltpu.VMEM((span, qw), BF16),
        pltpu.VMEM((pairs, span, 2 * kw), BF16),
        pltpu.VMEM((sp_count, heads, rows), BF16),
        pltpu.VMEM((sp_count, heads, rows), F32),
        pltpu.VMEM((pairs, local_heads, span), F32),
        pltpu.VMEM((span, local_heads), F32),
        pltpu.VMEM((local_heads, rows, head_dim), BF16),
        pltpu.SemaphoreType.DMA((3,)),
        pltpu.SemaphoreType.DMA((2, dp_count, 2)),
        pltpu.SemaphoreType.DMA((2, dp_count, 2)),
        pltpu.SemaphoreType.DMA((2,)),
        pltpu.SemaphoreType.DMA((sp_count,)),
        pltpu.SemaphoreType.DMA((sp_count,)),
        pltpu.SemaphoreType.DMA((pairs, 2)),
        pltpu.SemaphoreType.DMA((pairs, 2)),
        pltpu.SemaphoreType.DMA((local_heads,)),
        pltpu.SemaphoreType.DMA((local_heads,)),
    ]
    return kernel, scratch


def solution(mesh):
    sp_count, dp_count = mesh.shape["sp"], mesh.shape["dp"]

    def on_device(tokens, query_weight, key_weight, value_weight, forget_weight, forget_bias):
        rows, model = tokens.shape[1:]
        heads = forget_weight.shape[1]
        head_dim = query_weight.shape[1] // heads
        key_heads = key_weight.shape[1] // head_dim
        kernel, scratch = make_kernel(
            sp_count, dp_count, heads, key_heads, head_dim, rows, query_weight.shape[0])
        vmem = pl.BlockSpec(memory_space=pltpu.VMEM)
        hbm = pl.BlockSpec(memory_space=pl.ANY)
        mixed = pl.pallas_call(
            kernel,
            out_shape=jax.ShapeDtypeStruct((rows, heads * head_dim), BF16),
            in_specs=[vmem, hbm, hbm, hbm, vmem, pl.BlockSpec(memory_space=pltpu.SMEM)],
            out_specs=vmem,
            scratch_shapes=scratch,
            compiler_params=pltpu.CompilerParams(
                collective_id=0, has_side_effects=True, vmem_limit_bytes=48 * 2**20),
            name="mixer",
        )(tokens[0], query_weight, key_weight, value_weight, forget_weight.T, forget_bias)
        return mixed[None]

    placed = (P("dp", "sp", None), P("dp", None), P("dp", None), P("dp", None), P(), P())
    return jax.shard_map(
        on_device, mesh=mesh, in_specs=placed, out_specs=P("dp", "sp", None), check_vma=False
    )
```

time: 230 us -> 63.2 us (0.27)
  the two profiles are of different devices: /device:TPU:0 before, /device:TPU:27 now
where the time goes in v1:
time: 63.2 us; the launch traced here: 62.9 us
  Pallas kernels  56.3 us (89%)
  local copies, waits for them, and re-layouts  6.63 us (10%)
    pallas_call x1, Pallas kernels, on_device(): pl.pallas_call(kernel, out_shape=jax.ShapeDtypeStruct((rows, heads * head...  56.3 us
    unnamed x13, local copies, waits for them, and re-layouts  6.63 us

profile of v1, /device:TPU:27, one launch (start us, length us, event | category | flops | bytes accessed | tf_op | source)
XLA Modules:
  0.0 62.9 jit_solution(536692223788746913)
XLA Ops:
  0.0 0.0 copy-start.5
  0.0 0.7 %copy-done.5 = f32[16]{0:T(128)S(1)} copy-done((f32[16]{0:T(128)S(1)}, f32[16]{0:T(128)}, u32[]{:S(2)}) %copy-start.5) | copy-done | bytes 88
  0.7 0.0 copy-start
  0.7 1.2 %copy-done = bf16[256,2048]{1,0:T(8,128)(2,1)S(1)} copy-done((bf16[256,2048]{1,0:T(8,128)(2,1)S(1)}, bf16[256,2048]{1,0:T(8,128)(2,1)}, u32[]{:S(2)}) %copy-start) | copy-done | bytes 1048600
  1.9 0.0 copy-start.1
  1.9 1.1 %copy-done.1 = bf16[1,192,2048]{2,1,0:T(8,128)(2,1)S(1)} copy-done((bf16[1,192,2048]{2,1,0:T(8,128)(2,1)S(1)}, bf16[1,192,2048]{2,1,0:T(8,128)(2,1)}, u32[]{:S(2)}) %copy-start.1) | copy-done | bytes 786456
  3.0 0.0 copy-start.2
  3.0 0.9 %copy-done.2 = bf16[256,512]{1,0:T(8,128)(2,1)S(1)} copy-done((bf16[256,512]{1,0:T(8,128)(2,1)S(1)}, bf16[256,512]{1,0:T(8,128)(2,1)}, u32[]{:S(2)}) %copy-start.2) | copy-done | bytes 262168
  4.0 0.0 copy-start.3
  4.0 0.9 %copy-done.3 = bf16[256,512]{1,0:T(8,128)(2,1)S(1)} copy-done((bf16[256,512]{1,0:T(8,128)(2,1)S(1)}, bf16[256,512]{1,0:T(8,128)(2,1)}, u32[]{:S(2)}) %copy-start.3) | copy-done | bytes 262168
  4.9 0.0 copy-start.4
  4.9 0.8 %copy-done.4 = bf16[2048,16]{0,1:T(8,128)(2,1)S(1)} copy-done((bf16[2048,16]{0,1:T(8,128)(2,1)S(1)}, bf16[2048,16]{0,1:T(8,128)(2,1)}, u32[]{:S(2)}) %copy-start.4) | copy-done | bytes 65560
  5.8 56.3 %mixer.1 = bf16[192,2048]{1,0:T(8,128)(2,1)S(1)} custom-call(bf16[192,2048]{1,0:T(8,128)(2,1)S(1)} %bitcast.4, bf16[256,2048]{1,0:T(8,128)(2,1)S(1)} %copy-done, bf16[256,512]{1,0:T(8,128)(2,1)S(1)} %copy-done.2, bf16[256,512]{1,0:T(8,128)(2,1)S(1)} %copy-done.3, bf16[16,2048]{1,0:T(8,128)(2,1)S(1)} %bitcast.5, f32[16]{0:T(128)S(1)} %copy-done.5), custom_call_target="tpu_custom_call" | custom-call | tf_op jit(solution)/shard_map/mixer/pallas_call | solution.py:356
  62.0 0.9 %copy.8 = bf16[1,192,2048]{2,1,0:T(8,128)(2,1)} copy(bf16[1,192,2048]{2,1,0:T(8,128)(2,1)S(1)} %bitcast.3) | data formatting | bytes 1572864
Async XLA Ops:
  0.0 0.7 %copy-start.5 = (f32[16]{0:T(128)S(1)}, f32[16]{0:T(128)}, u32[]{:S(2)}) copy-start(f32[16]{0:T(128)} %bias_ref.1) | copy-start | bytes 196
  0.7 1.2 %copy-start = (bf16[256,2048]{1,0:T(8,128)(2,1)S(1)}, bf16[256,2048]{1,0:T(8,128)(2,1)}, u32[]{:S(2)}) copy-start(bf16[256,2048]{1,0:T(8,128)(2,1)} %wq_hbm.1) | copy-start | bytes 3145732
  1.9 1.1 %copy-start.1 = (bf16[1,192,2048]{2,1,0:T(8,128)(2,1)S(1)}, bf16[1,192,2048]{2,1,0:T(8,128)(2,1)}, u32[]{:S(2)}) copy-start(bf16[1,192,2048]{2,1,0:T(8,128)(2,1)} %param.6) | copy-start | bytes 2359300
  3.0 0.9 %copy-start.2 = (bf16[256,512]{1,0:T(8,128)(2,1)S(1)}, bf16[256,512]{1,0:T(8,128)(2,1)}, u32[]{:S(2)}) copy-start(bf16[256,512]{1,0:T(8,128)(2,1)} %wk_hbm.1) | copy-start | bytes 786436
  4.0 0.9 %copy-start.3 = (bf16[256,512]{1,0:T(8,128)(2,1)S(1)}, bf16[256,512]{1,0:T(8,128)(2,1)}, u32[]{:S(2)}) copy-start(bf16[256,512]{1,0:T(8,128)(2,1)} %wv_hbm.1) | copy-start | bytes 786436
  4.9 0.8 %copy-start.4 = (bf16[2048,16]{0,1:T(8,128)(2,1)S(1)}, bf16[2048,16]{0,1:T(8,128)(2,1)}, u32[]{:S(2)}) copy-start(bf16[2048,16]{0,1:T(8,128)(2,1)} %param.10) | copy-start | bytes 196612

commit v2 on v1

v2 whole, which is shorter than its diff:
```python
import math

import jax
import jax.numpy as jnp
from jax import lax
from jax.experimental import pallas as pl
from jax.experimental.pallas import tpu as pltpu
from jax.sharding import PartitionSpec as P

MESH = pl.DeviceIdType.MESH
F32 = jnp.float32
BF16 = jnp.bfloat16
NT = (((1,), (1,)), ((), ()))
LOG2E = math.log2(math.e)


def flip(index, mask):
    bit = 1
    while bit <= mask:
        if mask & bit:
            index = index + bit * (1 - 2 * ((index // bit) % 2))
        bit *= 2
    return index


def last_bit(mask, half):
    if mask & 1:
        return 1
    return 1 << (mask.bit_length() - 1) if half == 0 else mask & -mask


def make_kernel(sp_count, dp_count, heads, key_heads, head_dim, rows, shard):
    half_shard = shard // 2
    local_heads = heads // 2
    local_keys = key_heads // 2
    group = heads // key_heads
    kw = local_keys * head_dim
    qw = local_heads * head_dim
    pairs = sp_count // 2
    span = 2 * rows
    bits = [1 << i for i in range(dp_count.bit_length() - 1)]
    masks = sorted(range(1, dp_count), key=lambda m: (bin(m).count("1"), m))
    score_scale = head_dim ** (-0.5) * LOG2E
    chunks = 4 if rows % 64 == 0 else 1
    chunk = rows // chunks
    kvw = 2 * head_dim
    ow = group * head_dim
    tile = 256

    def kernel(x_ref, wq_hbm, wk_hbm, wv_hbm, fw_ref, bias_ref, out_ref,
               xpeer, wkv, wq, qbuf, kvbuf, gbuf, gwide, drow, dcol, osend,
               local_sem, w_send, w_recv, x_send, x_recv, g_send, g_recv, kv_send, kv_recv,
               o_send, o_recv):
        s = lax.axis_index("sp")
        d = lax.axis_index("dp")
        parity = s % 2
        pair = s // 2
        peer = s + 1 - 2 * parity

        def own_rows(index):
            return pl.ds(pl.multiple_of(index * shard, shard), shard)

        def local_copy(source, first, width, target, index):
            return pltpu.make_async_copy(
                source.at[:, pl.ds(pl.multiple_of(first, width), width)], target,
                local_sem.at[index])

        locals_ = []
        for kh in range(local_keys):
            for i, source in enumerate((wk_hbm, wv_hbm)):
                locals_.append(local_copy(
                    source, parity * kw + kh * head_dim, head_dim,
                    wkv.at[own_rows(d), pl.ds(kh * kvw + i * head_dim, head_dim)],
                    kh * 3 + i))
        for kh in range(local_keys):
            locals_.append(local_copy(
                wq_hbm, parity * qw + kh * ow, ow, wq.at[kh, own_rows(d), :], kh * 3 + 2))
        for copy in locals_:
            copy.start()

        barrier = pltpu.get_barrier_semaphore()
        for k in range(1, sp_count):
            pl.semaphore_signal(barrier, inc=1, device_id={"sp": (s + k) % sp_count},
                                device_id_type=MESH)
        for b in bits:
            pl.semaphore_signal(barrier, inc=1, device_id={"dp": flip(d, b)},
                                device_id_type=MESH)
        pl.semaphore_wait(barrier, sp_count - 1 + len(bits))

        def x_copy(c):
            where = pl.ds(c * chunk, chunk)
            return pltpu.make_async_remote_copy(
                x_ref.at[where, :], xpeer.at[where, :], x_send.at[c], x_recv.at[c],
                device_id={"sp": peer}, device_id_type=MESH)

        for c in range(chunks):
            x_copy(c).start()

        def shard_ref(part, where):
            return wkv.at[where, :] if part == 0 else wq.at[part - 1, where, :]

        def weight_copy(part, mask, half, bit):
            start = flip(d, mask) * shard + half * half_shard
            where = pl.ds(pl.multiple_of(start, half_shard), half_shard)
            there = mask | bit
            return pltpu.make_async_remote_copy(
                shard_ref(part, where), shard_ref(part, where),
                w_send.at[part, there, half], w_recv.at[part, there, half],
                device_id={"dp": flip(d, bit)}, device_id_type=MESH)

        sent = []

        def send(part, mask, half, bit):
            copy = weight_copy(part, mask, half, bit)
            copy.start()
            sent.append(copy)

        def arrive(part, mask, half):
            bit = last_bit(mask, half)
            start = flip(d, mask) * shard + half * half_shard
            where = pl.ds(pl.multiple_of(start, half_shard), half_shard)
            pltpu.make_async_remote_copy(
                shard_ref(part, where), shard_ref(part, where),
                w_send.at[part, mask, half], w_recv.at[part, mask, half],
                device_id={"dp": flip(d, bit)}, device_id_type=MESH).wait_recv()
            for b in reversed(bits):
                if not mask & b and last_bit(mask | b, half) == b:
                    send(part, mask, half, b)

        def first_half(bit):
            return 0 if bit == 2 else 1

        def direct(part, turn):
            for b in bits[1:] + bits[:1]:
                send(part, 0, (first_half(b) + turn) % 2, b)

        early = [(b, first_half(b)) for b in bits]
        late = [(b, 1 - first_half(b)) for b in bits]
        relayed = [(m, h) for m in masks if bin(m).count("1") > 1 for h in (0, 1)]

        for copy in locals_[:2 * local_keys]:
            copy.wait()
        direct(0, 0)
        direct(0, 1)
        for copy in locals_[2 * local_keys:]:
            copy.wait()
        for m, h in early:
            arrive(0, m, h)
        direct(1, 0)
        direct(1, 1)

        gate = lax.dot_general(fw_ref[...], x_ref[...], NT, preferred_element_type=F32)
        row_id = lax.broadcasted_iota(jnp.int32, (heads, 1), 0)
        bias = jnp.zeros((heads, 1), F32)
        for h in range(heads):
            bias = jnp.where(row_id == h, bias_ref[h], bias)
        gate = gate + bias
        log_gate = jnp.minimum(gate, 0.0) - jnp.log1p(jnp.exp(-jnp.abs(gate)))
        gbuf[s] = log_gate.astype(BF16)
        g_copies = []
        for k in range(1, sp_count):
            copy = pltpu.make_async_remote_copy(
                gbuf.at[s], gbuf.at[s], g_send.at[k], g_recv.at[s],
                device_id={"sp": (s + k) % sp_count}, device_id_type=MESH)
            copy.start()
            g_copies.append(copy)

        for m, h in late + relayed:
            arrive(0, m, h)

        def kv_copy(source_pair, target_pair, which, kh, piece):
            if piece == 0:
                where = pl.ds(pl.multiple_of(which * rows, rows), rows)
            else:
                first = which * rows + (piece - 1) * chunk
                where = pl.ds(pl.multiple_of(first, chunk), chunk)
            return pltpu.make_async_remote_copy(
                kvbuf.at[source_pair, kh, where, :], kvbuf.at[source_pair, kh, where, :],
                kv_send.at[target_pair, kh, piece], kv_recv.at[source_pair, kh, piece],
                device_id={"sp": target_pair * 2 + parity}, device_id_type=MESH)

        def kv_pieces():
            return [(parity, 0)] + [(1 - parity, 1 + c) for c in range(chunks)]

        def project_kv(which, piece):
            if piece == 0:
                source, first, count = x_ref[...], which * rows, rows
            else:
                source = xpeer[(piece - 1) * chunk:piece * chunk, :]
                first, count = which * rows + (piece - 1) * chunk, chunk
            where = pl.ds(pl.multiple_of(first, count), count)
            for kh in range(local_keys):
                kvbuf[pair, kh, where, :] = jnp.dot(
                    source, wkv[:, kh * kvw:(kh + 1) * kvw],
                    preferred_element_type=F32).astype(BF16)
                for j in range(1, pairs):
                    @pl.when(pair < j)
                    def _():
                        kv_copy(pair, j, which, kh, piece).start()

        def peer_chunk(c):
            x_copy(c).wait_recv()
            project_kv(1 - parity, 1 + c)

        project_kv(parity, 0)
        for m, h in early:
            arrive(1, m, h)
        for part in range(2, 1 + local_keys):
            direct(part, 0)
            direct(part, 1)
        for c in range(chunks - 1):
            peer_chunk(c)

        for k in range(1, sp_count):
            source = (s + k) % sp_count
            pltpu.make_async_remote_copy(
                gbuf.at[source], gbuf.at[source], g_send.at[k], g_recv.at[source],
                device_id={"sp": source}, device_id_type=MESH).wait_recv()
        gwide[...] = gbuf[...].astype(F32)
        mine = pl.ds(pl.multiple_of(parity * local_heads, local_heads), local_heads)
        up_row = lax.broadcasted_iota(jnp.int32, (rows, span), 0)
        up_col = lax.broadcasted_iota(jnp.int32, (rows, span), 1)
        upper_a = jnp.where(up_row <= up_col, 1.0, 0.0).astype(BF16)
        upper_b = jnp.where(up_row + rows <= up_col, 1.0, 0.0).astype(BF16)
        low_row = lax.broadcasted_iota(jnp.int32, (span, rows), 0) + pair * span
        low_col = lax.broadcasted_iota(jnp.int32, (span, rows), 1)
        before = jnp.zeros((local_heads, 1), F32)
        column = jnp.zeros((span, local_heads), F32)
        for j in range(pairs):
            wide_a = gwide[2 * j, mine, :]
            wide_b = gwide[2 * j + 1, mine, :]
            gate_a = wide_a.astype(BF16)
            gate_b = wide_b.astype(BF16)
            inside = (jnp.dot(gate_a, upper_a, preferred_element_type=F32)
                      + jnp.dot(gate_b, upper_b, preferred_element_type=F32))
            sums = (inside + before) * LOG2E
            for kh in range(local_keys):
                drow[j, kh] = sums[kh * group:(kh + 1) * group]
            before = (before + jnp.sum(wide_a, axis=1, keepdims=True)
                      + jnp.sum(wide_b, axis=1, keepdims=True))
            for block, gates in ((2 * j, gate_a), (2 * j + 1, gate_b)):
                lower = jnp.where(low_col + block * rows <= low_row, 1.0, 0.0).astype(BF16)
                column = column + lax.dot_general(lower, gates, NT, preferred_element_type=F32)
        column = column * LOG2E
        for kh in range(local_keys):
            dcol[kh] = column[:, kh * group:(kh + 1) * group]

        peer_chunk(chunks - 1)

        def project_q(source, block, kh):
            where = pl.ds(pl.multiple_of(block * rows, rows), rows)

            def one(c, carry):
                cols = pl.ds(pl.multiple_of(c * tile, tile), tile)
                qbuf[kh, where, cols] = jnp.dot(
                    source[...], wq[kh, :, cols], preferred_element_type=F32).astype(BF16)
                return carry

            lax.fori_loop(0, ow // tile, one, 0)

        def out_copy(kh, half):
            cols = pl.ds(pl.multiple_of(half * qw + kh * ow, ow), ow)
            return pltpu.make_async_remote_copy(
                osend.at[kh], out_ref.at[:, cols], o_send.at[kh], o_recv.at[kh],
                device_id={"sp": peer}, device_id_type=MESH)

        def attend(block, kh, awaited):
            where = pl.ds(pl.multiple_of(block * rows, rows), rows)
            row = lax.broadcasted_iota(jnp.int32, (rows, span), 0) + block * rows
            col = lax.broadcasted_iota(jnp.int32, (rows, span), 1)
            allowed = col <= row

            def scores(j, g):
                query = qbuf[kh, where, g * head_dim:(g + 1) * head_dim]
                key = kvbuf[j, kh, :, :head_dim]
                raw = lax.dot_general(query, key, NT, preferred_element_type=F32)
                return raw * score_scale + dcol[kh, where, g:g + 1] - drow[j, kh, g:g + 1, :]

            def values(j):
                return kvbuf[j, kh, :, head_dim:]

            states = []
            for g in range(group):
                sc = jnp.where(allowed, scores(pair, g), -jnp.inf)
                top = jnp.max(sc, axis=1, keepdims=True)
                weight = jnp.exp2(sc - top)
                total = jnp.sum(weight, axis=1, keepdims=True)
                acc = jnp.dot(weight.astype(BF16), values(pair), preferred_element_type=F32)
                states.append((top, total, acc))

            def earlier(j, states):
                if awaited:
                    for which, piece in kv_pieces():
                        kv_copy(j, pair, which, kh, piece).wait_recv()
                after = []
                for g in range(group):
                    top, total, acc = states[g]
                    sc = scores(j, g)
                    new_top = jnp.maximum(top, jnp.max(sc, axis=1, keepdims=True))
                    keep = jnp.exp2(top - new_top)
                    weight = jnp.exp2(sc - new_top)
                    total = total * keep + jnp.sum(weight, axis=1, keepdims=True)
                    acc = acc * keep + jnp.dot(
                        weight.astype(BF16), values(j), preferred_element_type=F32)
                    after.append((new_top, total, acc))
                return tuple(after)

            states = lax.fori_loop(0, pair, earlier, tuple(states))
            return [(acc / total).astype(BF16) for _, total, acc in states]

        for m, h in late + relayed:
            arrive(1, m, h)
        for kh in range(local_keys):
            project_q(xpeer, 1 - parity, kh)
            for m, h in early if kh + 1 < local_keys else ():
                arrive(kh + 2, m, h)
            for g, result in enumerate(attend(1 - parity, kh, True)):
                osend[kh, :, g * head_dim:(g + 1) * head_dim] = result
            out_copy(kh, parity).start()
            for m, h in late + relayed if kh + 1 < local_keys else ():
                arrive(kh + 2, m, h)
        for kh in range(local_keys):
            project_q(x_ref, parity, kh)
            for g, result in enumerate(attend(parity, kh, False)):
                first = parity * qw + kh * ow + g * head_dim
                out_ref[:, pl.ds(pl.multiple_of(first, head_dim), head_dim)] = result

        for c in range(chunks):
            x_copy(c).wait_send()
        for copy in sent + g_copies:
            copy.wait_send()
        for j in range(1, pairs):
            @pl.when(pair < j)
            def _():
                for kh in range(local_keys):
                    for which, piece in kv_pieces():
                        kv_copy(pair, j, which, kh, piece).wait_send()
        for kh in range(local_keys):
            out_copy(kh, parity).wait_send()
            out_copy(kh, 1 - parity).wait_recv()

    model = shard * dp_count
    scratch = [
        pltpu.VMEM((rows, model), BF16),
        pltpu.VMEM((model, 2 * kw), BF16),
        pltpu.VMEM((local_keys, model, ow), BF16),
        pltpu.VMEM((local_keys, span, ow), BF16),
        pltpu.VMEM((pairs, local_keys, span, kvw), BF16),
        pltpu.VMEM((sp_count, heads, rows), BF16),
        pltpu.VMEM((sp_count, heads, rows), F32),
        pltpu.VMEM((pairs, local_keys, group, span), F32),
        pltpu.VMEM((local_keys, span, group), F32),
        pltpu.VMEM((local_keys, rows, group * head_dim), BF16),
        pltpu.SemaphoreType.DMA((3 * local_keys,)),
        pltpu.SemaphoreType.DMA((1 + local_keys, dp_count, 2)),
        pltpu.SemaphoreType.DMA((1 + local_keys, dp_count, 2)),
        pltpu.SemaphoreType.DMA((chunks,)),
        pltpu.SemaphoreType.DMA((chunks,)),
        pltpu.SemaphoreType.DMA((sp_count,)),
        pltpu.SemaphoreType.DMA((sp_count,)),
        pltpu.SemaphoreType.DMA((pairs, local_keys, 1 + chunks)),
        pltpu.SemaphoreType.DMA((pairs, local_keys, 1 + chunks)),
        pltpu.SemaphoreType.DMA((local_keys,)),
        pltpu.SemaphoreType.DMA((local_keys,)),
    ]
    return kernel, scratch


def solution(mesh):
    sp_count, dp_count = mesh.shape["sp"], mesh.shape["dp"]

    def on_device(tokens, query_weight, key_weight, value_weight, forget_weight, forget_bias):
        rows, model = tokens.shape[1:]
        heads = forget_weight.shape[1]
        head_dim = query_weight.shape[1] // heads
        key_heads = key_weight.shape[1] // head_dim
        kernel, scratch = make_kernel(
            sp_count, dp_count, heads, key_heads, head_dim, rows, query_weight.shape[0])
        vmem = pl.BlockSpec(memory_space=pltpu.VMEM)
        hbm = pl.BlockSpec(memory_space=pl.ANY)
        mixed = pl.pallas_call(
            kernel,
            out_shape=jax.ShapeDtypeStruct((rows, heads * head_dim), BF16),
            in_specs=[vmem, hbm, hbm, hbm, vmem, pl.BlockSpec(memory_space=pltpu.SMEM)],
            out_specs=vmem,
            scratch_shapes=scratch,
            compiler_params=pltpu.CompilerParams(
                collective_id=0, has_side_effects=True, vmem_limit_bytes=63 * 2**20),
            name="mixer",
        )(tokens[0], query_weight, key_weight, value_weight, forget_weight.T, forget_bias)
        return mixed[None]

    placed = (P("dp", "sp", None), P("dp", None), P("dp", None), P("dp", None), P(), P())
    return jax.shard_map(
        on_device, mesh=mesh, in_specs=placed, out_specs=P("dp", "sp", None), check_vma=False
    )
```

time: 63.2 us -> 55.7 us (0.88)
  local copies, waits for them, and re-layouts: 6.63 us -> 2.09 us
  Pallas kernels: 56.3 us -> 53.2 us
    unnamed x13 -> x1, local copies, waits for them, and re-layouts: 6.63 us -> 2.09 us
    pallas_call x1, Pallas kernels: 56.3 us -> 53.2 us  [on_device(): pl.pallas_call(kernel, out_shape=jax.ShapeDtypeStruct((rows, heads * head...]
where the time goes in v2:
time: 55.7 us; the launch traced here: 55.3 us
  Pallas kernels  53.2 us (96%)
  local copies, waits for them, and re-layouts  2.09 us (4%)
    pallas_call x1, Pallas kernels, on_device(): pl.pallas_call(kernel, out_shape=jax.ShapeDtypeStruct((rows, heads * head...  53.2 us
    unnamed x1, local copies, waits for them, and re-layouts  2.09 us

profile of v2, /device:TPU:27, one launch (start us, length us, event | category | flops | bytes accessed | tf_op | source)
XLA Modules:
  0.0 55.3 jit_solution(1669678562746366712)
XLA Ops:
  0.0 53.2 %mixer.1 = bf16[192,2048]{1,0:T(8,128)(2,1)} custom-call(bf16[192,2048]{1,0:T(8,128)(2,1)} %bitcast.4, bf16[256,2048]{1,0:T(8,128)(2,1)} %wq_hbm.1, bf16[256,512]{1,0:T(8,128)(2,1)} %wk_hbm.1, bf16[256,512]{1,0:T(8,128)(2,1)} %wv_hbm.1, bf16[16,2048]{1,0:T(8,128)(2,1)} %bitcast.5, f32[16]{0:T(128)} %bias_ref.1), custom_call_target="tpu_custom_call" | custom-call | tf_op jit(solution)/shard_map/mixer/pallas_call | solution.py:381
  53.2 2.1 %copy.8 = bf16[1,192,2048]{2,1,0:T(8,128)(2,1)} copy(bf16[1,192,2048]{2,1,0:T(8,128)(2,1)} %bitcast.3) | data formatting | bytes 1572864
